TPU v7x, 32 devices: a whole 2x2x4 slice. The times are simulated.
32 devices in a mesh: sp: 8 (over z, x), tp: 4 (over y, core).
Axes of the slice: x: 2, y: 2, z: 4, core: 2. Of those that a mesh axis runs over, the one named last changes fastest.
Arguments:
- residual: bfloat16 [6144, 2048], P('sp'), may hold values from -6 to 6
- queries: bfloat16 [6144, 1024], P('sp', 'tp'), may hold values from -12 to 12
- keys: bfloat16 [6144, 512], P('sp', 'tp'), may hold values from -6 to 6
- values: bfloat16 [6144, 512], P('sp', 'tp'), may hold values from -36 to 36
- segments: int32 [6144], P('sp'), may hold values from 0 to 3, never falling along the last dimension, each value on 1 to 3072 neighbouring positions
- sink: float32 [16], P('tp'), may hold values from 3 to 7
- out_weight: bfloat16 [1024, 2048], replicated, may hold values from -0.1875 to 0.1875
- norm_gain_one: float32 [2048], replicated, may hold values from 0.1 to 1.9
- group: int32 [6144], P('sp'), may hold values from 0 to 3, as said below
- member: int32 [6144, 2], P('sp'), may hold values from 0 to 7, as said below
- route_weight: float32 [6144, 2], P('sp'), may hold values from 0.25 to 1
- gate_weight: bfloat16 [32, 2048, 1024], P('sp', None, 'tp'), may hold values from -0.125 to 0.125
- up_weight: bfloat16 [32, 2048, 1024], P('sp', None, 'tp'), may hold values from -0.125 to 0.125
- down_weight: bfloat16 [32, 1024, 2048], P('sp', None, 'tp'), may hold values from -0.1875 to 0.1875
- norm_gain_two: float32 [2048], P('tp'), may hold values from 0.1 to 1.9
Outputs:
- output: bfloat16 [6144, 2048], P('sp', 'tp')
Inputs may be any that keep to these rules, and one draw needn't show every extreme that they name: In every aligned block of 192 rows no expert (group * 8 + member) is named by more than 24 rows, and one expert, the same in all blocks of a draw, is named by exactly 24 rows of every block. `member`: the 2 members of a row differ.
All inputs are finite; a program needn't handle non-finite values.
Results may differ from a plain program's by a relative error of at most 0.0059.
Values may be sent and summed in bfloat16 or wider, within the bound.
A program may use at most 128 MiB of HBM per device.

v0:
```python
import math
import jax
import jax.numpy as jnp
from jax import lax
from jax.sharding import PartitionSpec as P

HEAD_DIM = 64
HALF = 128
PER_GROUP = 8
ALPHA = 2.0**0.25
EPS = 1e-05


def with_halo(block, sides, width):
    for axis, dim in sides:
        count = lax.axis_size(axis)
        forward = [(i, i + 1) for i in range(count - 1)]
        backward = [(target, source) for source, target in forward]
        low = lax.ppermute(
            lax.slice_in_dim(block, block.shape[dim] - width, None, axis=dim), axis, forward
        )
        high = lax.ppermute(lax.slice_in_dim(block, 0, width, axis=dim), axis, backward)
        block = jnp.concatenate([low, block, high], axis=dim)
    return block


def layer_norm(summed, norm_gain):
    mean_value = jnp.mean(summed, -1, keepdims=True)
    variance = jnp.mean(jnp.square(summed - mean_value), -1, keepdims=True)
    return ((summed - mean_value) * lax.rsqrt(variance + EPS) * norm_gain).astype(jnp.bfloat16)


def shards(
    residual,
    queries,
    keys,
    values,
    segments,
    sink,
    out_weight,
    norm_gain_one,
    group,
    member,
    route_weight,
    gate_weight,
    up_weight,
    down_weight,
    norm_gain_two,
):
    row_count = queries.shape[0]
    sp_size = lax.axis_size("sp")
    tp_size = lax.axis_size("tp")
    kv_local = keys.shape[1] // HEAD_DIM
    heads_local = queries.shape[1] // HEAD_DIM
    group_size = heads_local // kv_local
    seq_total = row_count * sp_size
    seq_start = lax.axis_index("sp") * row_count
    joined = jnp.concatenate([keys, values], axis=1)
    padded, seg_padded = (
        with_halo(joined, (("sp", 0),), HALF),
        with_halo(segments, (("sp", 0),), HALF),
    )
    query_block = math.gcd(row_count, 512)
    key_span = query_block + 2 * HALF
    offsets = jnp.arange(key_span)[None, :] - HALF - jnp.arange(query_block)[:, None]
    in_band = jnp.abs(offsets) <= HALF
    sink_heads = sink.reshape(kv_local, group_size, 1, 1)
    query_heads = queries.reshape(row_count, kv_local, group_size, HEAD_DIM)
    key_cols = kv_local * HEAD_DIM
    pieces = []
    for number in range(row_count // query_block):
        row_low = number * query_block
        query_rows = query_heads[row_low : row_low + query_block]
        kv_rows = padded[row_low : row_low + key_span]
        key_part = kv_rows[:, :key_cols].reshape(key_span, kv_local, HEAD_DIM)
        value_part = kv_rows[:, key_cols:].reshape(key_span, kv_local, HEAD_DIM)
        key_place = seq_start + row_low - HALF + jnp.arange(key_span)
        inside = (key_place >= 0) & (key_place < seq_total)
        same_doc = (
            segments[row_low : row_low + query_block, None]
            == seg_padded[None, row_low : row_low + key_span]
        )
        allowed = in_band & same_doc & inside[None, :]
        scores = jnp.einsum(
            "qkgd,ckd->kgqc", query_rows, key_part, preferred_element_type=jnp.float32
        ) * HEAD_DIM ** (-0.5)
        masked = jnp.where(allowed, scores, -1e30)
        peak = jnp.maximum(jnp.max(masked, -1, keepdims=True), sink_heads)
        raised = jnp.where(allowed, jnp.exp(masked - peak), 0.0)
        denominator = jnp.sum(raised, -1, keepdims=True) + jnp.exp(sink_heads - peak)
        weights = (raised / denominator).astype(jnp.bfloat16)
        attended_part = jnp.einsum(
            "kgqc,ckd->qkgd", weights, value_part, preferred_element_type=jnp.float32
        )
        pieces.append(
            attended_part.reshape(query_block, heads_local * HEAD_DIM).astype(jnp.bfloat16)
        )
    attended = jnp.concatenate(pieces, 0)
    width = out_weight.shape[1]
    weight_rows = out_weight
    mixed = jnp.dot(
        lax.all_gather(attended, "tp", axis=1, tiled=True),
        weight_rows,
        preferred_element_type=jnp.float32,
    )
    pre_one = ALPHA * residual.astype(jnp.float32) + mixed
    normed = layer_norm(pre_one, norm_gain_one)
    experts_local = gate_weight.shape[0]
    expert_count = experts_local * sp_size
    picks_count = member.shape[1]
    block_rows = row_count // tp_size
    capacity = max(2, block_rows // 8)
    expert_ids = (group[:, None] * PER_GROUP + member).reshape(tp_size, block_rows * picks_count)
    onehot_table = (expert_ids[:, :, None] == jnp.arange(expert_count)[None, None, :]).astype(
        jnp.int32
    )
    ranks = jnp.sum((jnp.cumsum(onehot_table, 1) - 1) * onehot_table, 2)
    owner = expert_ids // experts_local
    local_ids = expert_ids % experts_local
    block_ids = jnp.arange(tp_size)[:, None]
    slot_all = ((local_ids * sp_size + owner) * tp_size + block_ids) * capacity + ranks
    copy_rows = (
        jnp.arange(row_count * picks_count).reshape(tp_size, block_rows * picks_count)
        // picks_count
    )
    extended = jnp.concatenate([normed, jnp.zeros((1, width), jnp.bfloat16)], 0)
    tp_place = lax.axis_index("tp")
    slot_own_base = (local_ids * sp_size + owner) * capacity + ranks
    own_slots = lax.dynamic_index_in_dim(slot_own_base, tp_place, 0, keepdims=False)
    own_rows = lax.dynamic_index_in_dim(copy_rows, tp_place, 0, keepdims=False)
    slot_count = experts_local * sp_size * capacity
    source = jnp.full((slot_count,), row_count, jnp.int32).at[own_slots].set(own_rows)
    outgoing = extended[source].reshape(experts_local, sp_size, capacity, width)
    received = lax.all_to_all(outgoing, "sp", split_axis=1, concat_axis=1, tiled=True)
    arrived = lax.all_gather(received, "tp", axis=2, tiled=True)
    expert_rows = arrived.reshape(experts_local, sp_size * tp_size * capacity, width)
    gate_part = jnp.einsum(
        "esd,edf->esf", expert_rows, gate_weight, preferred_element_type=jnp.float32
    )
    up_part = jnp.einsum("esd,edf->esf", expert_rows, up_weight, preferred_element_type=jnp.float32)
    hidden = (jax.nn.silu(gate_part) * up_part).astype(jnp.bfloat16)
    column_width = down_weight.shape[2]
    weight_rows = down_weight
    produced = jnp.einsum(
        "esf,efc->esc",
        lax.all_gather(hidden, "tp", axis=2, tiled=True),
        weight_rows,
        preferred_element_type=jnp.float32,
    ).astype(jnp.bfloat16)
    returned = lax.all_to_all(
        produced.reshape(experts_local, sp_size, tp_size * capacity, column_width),
        "sp",
        split_axis=1,
        concat_axis=1,
        tiled=True,
    )
    result_rows = returned.reshape(-1, column_width)
    picked = result_rows[slot_all.reshape(row_count, picks_count)]
    combined = jnp.sum(route_weight[:, :, None] * picked.astype(jnp.float32), 1)
    column_start = lax.axis_index("tp") * column_width
    normed_part = lax.dynamic_slice_in_dim(normed, column_start, column_width, 1)
    pre_two = ALPHA * normed_part.astype(jnp.float32) + combined
    sums, squares = lax.psum((jnp.sum(pre_two, -1), jnp.sum(pre_two * pre_two, -1)), "tp")
    mean_value = (sums / width)[:, None]
    variance = (squares / width)[:, None] - mean_value * mean_value
    return ((pre_two - mean_value) * lax.rsqrt(variance + EPS) * norm_gain_two).astype(jnp.bfloat16)


def solution(mesh):
    in_specs = (
        P("sp", None),
        P("sp", "tp"),
        P("sp", "tp"),
        P("sp", "tp"),
        P("sp"),
        P("tp"),
        P(),
        P(),
        P("sp"),
        P("sp", None),
        P("sp", None),
        P("sp", None, "tp"),
        P("sp", None, "tp"),
        P("sp", None, "tp"),
        P("tp"),
    )
    out_specs = P("sp", "tp")
    return jax.shard_map(shards, mesh=mesh, in_specs=in_specs, out_specs=out_specs, check_vma=False)
```

profile of v0, /device:TPU:0, one launch (start us, length us, event | category | flops | bytes accessed | tf_op | source)
XLA Modules:
  0.0 423.6 jit_solution(6903600422677034529)
XLA Ops:
  6.6 0.8 fusion.54
  7.4 4.9 %collective-permute-start.1 = (s32[128]{0:T(128)S(1)}, s32[128]{0:T(128)S(1)}, u32[]{:S(2)}, u32[]{:S(2)}) collective-permute-start(s32[128]{0:T(128)S(1)} %get-tuple-element.30), channel_id=1, source_target_pairs={{0,4},{4,8},{8,12},{12,16},{16,20},{20,24},{24,28},{1,5},{5,9},{9,... | collective-permute-start | bytes 1544 | tf_op jit(solution)/shard_map/ppermute | solution.py:19
  12.3 1.3 collective-permute-start.3
  13.6 1.0 constant_dynamic-update-slice_fusion.1
  14.5 1.0 constant_dynamic-update-slice_fusion
  15.5 0.6 fusion.52
  16.1 4.5 %collective-permute-start = (bf16[128,256]{1,0:T(8,128)(2,1)}, bf16[128,256]{1,0:T(8,128)(2,1)S(1)}, u32[]{:S(2)}, u32[]{:S(2)}) collective-permute-start(bf16[128,256]{1,0:T(8,128)(2,1)} %get-tuple-element.20), channel_id=1, source_target_pairs={{0,4},{4,8},{8,12},{12,16},{16,20},{20,24},{24,28},{1,5},{5,9},{9,... | collective-permute-start | bytes 196616 | tf_op jit(solution)/shard_map/ppermute | solution.py:19
  20.7 1.3 collective-permute-start.2
  22.0 0.7 slice.96
  22.7 0.8 fusion.55
  23.5 1.1 fusion.51
  24.8 0.8 copy.52
  26.0 0.7 and_and_fusion.2
  27.2 0.6 copy-done.7
  27.9 1.5 pad_maximum_fusion.3
  29.4 1.0 copy.47
  30.4 0.8 copy.46
  32.6 0.5 fusion.2
  33.2 0.8 convolution_convert_fusion.3
  35.1 0.8 convolution_convert_fusion.2
  36.0 0.7 convolution_convert_fusion.1
  36.8 0.8 pad_maximum_fusion
  38.5 3.5 reduce-window.6
  42.6 3.1 scatter_custom_fusion
  45.7 14.9 %all-gather.4.cloned.1.call-done = bf16[768,1024]{0,1:T(8,128)(2,1)} async-done(((bf16[768,256]{0,1:T(8,128)(2,1)}), bf16[768,1024]{0,1:T(8,128)(2,1)}) %all-gather.4.cloned.1.call-update) | async-done | bytes 1572880 | tf_op jit(solution)/shard_map/all_gather | solution.py:102
  60.6 7.8 %fusion.56 = (f32[768]{0:T(1024)S(1)}, f32[768,2048]{1,0:T(8,128)S(1)}) fusion(bf16[768,1024]{0,1:T(8,128)(2,1)} %all-gather.4.cloned.1.call-done, bf16[1024,2048]{1,0:T(8,128)(2,1)} %param.21, bf16[768,2048]{1,0:T(8,128)(2,1)} %param.15), kind=kOutput, calls=%fused_computation.146 | convolution fusion | flops 3227516160 | bytes 15207424 | tf_op jit(solution)/shard_map/dot_general | solution.py:101
  68.5 0.8 multiply_reduce_fusion
  69.3 0.9 multiply_convert_fusion
  70.1 1.7 copy-done
  72.0 4.3 %gather_fusion = bf16[768,2048]{1,0:T(8,128)(2,1)} fusion(bf16[769,2048]{1,0:T(8,128)(2,1)S(1)} %concatenate.29, s32[1024]{0:T(1024)S(1)} %pad_clamp_fusion.1), kind=kCustom, calls=%fused_computation | custom fusion | bytes 6294528 | tf_op jit(solution)/shard_map/gather | solution.py:133
  76.3 2.3 copy.63
  78.6 76.5 %all_to_all.10 = bf16[4,8,24,2048]{3,2,0,1:T(8,128)(2,1)} all-to-all(bf16[4,8,24,2048]{3,2,0,1:T(8,128)(2,1)S(1)} %copy.63), channel_id=1, replica_groups=mesh['sp'=8,'tp'=4] {'sp'}, dimensions={1} | all-to-all | bytes 6291456 | tf_op jit(solution)/shard_map/all_to_all | solution.py:134
  155.4 80.1 %all-gather.6.cloned.1.call-done = bf16[4,8,96,2048]{3,2,0,1:T(8,128)(2,1)} async-done(((bf16[4,8,24,2048]{3,2,0,1:T(8,128)(2,1)}), bf16[4,8,96,2048]{3,2,0,1:T(8,128)(2,1)}) %all-gather.6.cloned.1.call-update) | async-done | bytes 12582928 | tf_op jit(solution)/shard_map/all_gather | solution.py:135
  235.5 6.4 %copy.64 = bf16[4,8,96,2048]{3,2,1,0:T(8,128)(2,1)S(1)} copy(bf16[4,8,96,2048]{3,2,0,1:T(8,128)(2,1)} %all-gather.6.cloned.1.call-done) | data formatting | bytes 25165824 | tf_op jit(solution)/shard_map/all_gather | solution.py:135
  241.9 5.1 %fusion.57 = f32[4,768,256]{2,1,0:T(8,128)} fusion(bf16[4,768,2048]{2,1,0:T(8,128)(2,1)S(1)} %bitcast.120, bf16[4,2048,256]{2,1,0:T(8,128)(2,1)S(1)} %copy-done.14), kind=kOutput, calls=%fused_computation.147 | convolution fusion | flops 3221225472 | bytes 19922944 | tf_op jit(solution)/shard_map/esd,edf->esf/dot_general | solution.py:137
  247.1 7.4 %multiply_convert_fusion.1 = bf16[4,768,256]{2,1,0:T(8,128)(2,1)} fusion(f32[4,768,256]{2,1,0:T(8,128)} %fusion.57, bf16[4,768,2048]{2,1,0:T(8,128)(2,1)S(1)} %bitcast.121, bf16[4,2048,256]{2,1,0:T(8,128)(2,1)} %param.27), kind=kOutput, calls=%fused_computation.7 | convolution fusion | flops 3225944064 | bytes 21495808 | tf_op jit(solution)/shard_map/esd,edf->esf/dot_general | solution.py:140
  254.5 47.3 %all-gather.8.cloned.1.call-done = bf16[4,768,1024]{2,1,0:T(8,128)(2,1)} async-done(((bf16[4,768,256]{2,1,0:T(8,128)(2,1)}), bf16[4,768,1024]{2,1,0:T(8,128)(2,1)}) %all-gather.8.cloned.1.call-update) | async-done | bytes 6291472 | tf_op jit(solution)/shard_map/all_gather | solution.py:146
  301.8 7.4 %convolution_convert_fusion = bf16[4,768,512]{2,1,0:T(8,128)(2,1)S(1)} fusion(bf16[4,768,1024]{2,1,0:T(8,128)(2,1)} %all-gather.8.cloned.1.call-done, bf16[4,1024,512]{2,1,0:T(8,128)(2,1)} %param.28), kind=kOutput, calls=%fused_computation.8 | convolution fusion | flops 3222798336 | bytes 13631488 | tf_op jit(solution)/shard_map/esf,efc->esc/dot_general | solution.py:144
  309.3 2.0 copy.65
  311.3 5.7 %all-to-all-start.1 = ((bf16[4,8,96,512]{3,2,0,1:T(8,128)(2,1)}), bf16[4,8,96,512]{3,2,0,1:T(8,128)(2,1)}, u32[]{:S(2)}, u32[]{:S(2)}) async-start(bf16[4,8,96,512]{3,2,0,1:T(8,128)(2,1)} %copy.65), calls=%async_computation.1 | async-start | bytes 6291456 | tf_op jit(solution)/shard_map/all_to_all | solution.py:150
  318.3 69.8 %all-to-all-done.1 = bf16[4,8,96,512]{3,2,0,1:T(8,128)(2,1)} async-done(((bf16[4,8,96,512]{3,2,0,1:T(8,128)(2,1)}), bf16[4,8,96,512]{3,2,0,1:T(8,128)(2,1)}, u32[]{:S(2)}, u32[]{:S(2)}) %all-to-all-start.1) | async-done | bytes 3145760 | tf_op jit(solution)/shard_map/all_to_all | solution.py:150
  388.1 2.2 copy.66
  390.4 5.4 %gather_fusion.1 = bf16[1536,512]{1,0:T(8,128)(2,1)} fusion(bf16[3072,512]{1,0:T(8,128)(2,1)S(1)} %bitcast.119, s32[2048]{0:T(1024)S(1)} %pad_clamp_fusion), kind=kCustom, calls=%fused_computation.1 | custom fusion | bytes 3151872 | tf_op jit(solution)/shard_map/gather | solution.py:158
  395.8 4.8 %reshape.238 = f32[768,2,512]{2,1,0:T(2,128)} reshape(bf16[1536,512]{1,0:T(8,128)(2,1)} %gather_fusion.1) | data formatting | bytes 4718592 | tf_op jit(solution)/shard_map/convert_element_type | solution.py:159
  400.6 6.1 %multiply_reduce_fusion.1 = f32[768,512]{1,0:T(8,128)S(1)} fusion(f32[768,2,512]{2,1,0:T(2,128)} %reshape.238, f32[768,2]{1,0:T(8,128)S(1)} %copy.58), kind=kLoop, calls=%fused_computation.6 | loop fusion | flops 1179648 | bytes 4724736 | tf_op jit(solution)/shard_map/reduce_sum | solution.py:159
  406.7 1.2 copy-done.2
  408.3 6.1 %all-reduce.1 = (f32[768]{0:T(1024)S(1)}, f32[768]{0:T(1024)S(1)}) all-reduce(f32[768]{0:T(1024)S(1)} %get-tuple-element.6, f32[768]{0:T(1024)S(1)} %get-tuple-element.5), channel_id=1, replica_groups=mesh['sp'=8,'tp'=4] {'tp'}, use_global_device_ids=true, to_apply=%region_16.17 | all-reduce | flops 1536 | bytes 12288 | tf_op jit(solution)/shard_map/psum | solution.py:163
  414.4 2.6 multiply_convert_fusion.2
  (97 shorter events, 7.7 us)
Async XLA Ops:
  6.5 19.4 %copy-start.8 = (s32[768]{0:T(1024)S(1)}, s32[768]{0:T(1024)}, u32[]{:S(2)}) copy-start(s32[768]{0:T(1024)} %param.19) | copy-start | bytes 9220
  6.5 18.1 %slice-start = ((bf16[768,128]{1,0:T(8,128)(2,1)}), bf16[512,128]{1,0:T(8,128)(2,1)S(1)}, s32[]{:S(2)}) async-start(bf16[768,128]{1,0:T(8,128)(2,1)} %param.17), calls=%async_computation.5 | async-start | bytes 262144 | tf_op jit(solution)/shard_map/slice | solution.py:75
  6.5 18.3 %slice-start.1 = ((bf16[768,128]{1,0:T(8,128)(2,1)}), bf16[512,128]{1,0:T(8,128)(2,1)S(1)}, s32[]{:S(2)}) async-start(bf16[768,128]{1,0:T(8,128)(2,1)} %param.18), calls=%async_computation.6 | async-start | bytes 262144 | tf_op jit(solution)/shard_map/slice | solution.py:76
  6.5 18.0 %copy-start.15 = (f32[4]{0:T(128)S(1)}, f32[4]{0:T(128)}, u32[]{:S(2)}) copy-start(f32[4]{0:T(128)} %param.20) | copy-start | bytes 52
  6.5 54.1 %all-gather.4.cloned.1.call-start = ((), (), s32[]{:S(2)}) async-start(), calls=%async_computation.2 | async-start | bytes 1966080 | tf_op jit(solution)/shard_map/all_gather | solution.py:102
  7.4 18.5 %collective-permute-start.1 = (s32[128]{0:T(128)S(1)}, s32[128]{0:T(128)S(1)}, u32[]{:S(2)}, u32[]{:S(2)}) collective-permute-start(s32[128]{0:T(128)S(1)} %get-tuple-element.30), channel_id=1, source_target_pairs={{0,4},{4,8},{8,12},{12,16},{16,20},{20,24},{24,28},{1,5},{5,9},{9,... | collective-permute-start | bytes 1544 | tf_op jit(solution)/shard_map/ppermute | solution.py:19
  12.3 13.6 %collective-permute-start.3 = (s32[128]{0:T(128)S(1)}, s32[128]{0:T(128)S(1)}, u32[]{:S(2)}, u32[]{:S(2)}) collective-permute-start(s32[128]{0:T(128)S(1)} %get-tuple-element.31), channel_id=1, source_target_pairs={{4,0},{8,4},{12,8},{16,12},{20,16},{24,20},{28,24},{5,1},{9,5},{13... | collective-permute-start | bytes 1544 | tf_op jit(solution)/shard_map/ppermute | solution.py:22
  16.1 11.1 %collective-permute-start = (bf16[128,256]{1,0:T(8,128)(2,1)}, bf16[128,256]{1,0:T(8,128)(2,1)S(1)}, u32[]{:S(2)}, u32[]{:S(2)}) collective-permute-start(bf16[128,256]{1,0:T(8,128)(2,1)} %get-tuple-element.20), channel_id=1, source_target_pairs={{0,4},{4,8},{8,12},{12,16},{16,20},{20,24},{24,28},{1,5},{5,9},{9,... | collective-permute-start | bytes 196616 | tf_op jit(solution)/shard_map/ppermute | solution.py:19
  20.7 7.2 %collective-permute-start.2 = (bf16[128,256]{1,0:T(8,128)(2,1)S(1)}, bf16[128,256]{1,0:T(8,128)(2,1)}, u32[]{:S(2)}, u32[]{:S(2)}) collective-permute-start(bf16[128,256]{1,0:T(8,128)(2,1)S(1)} %get-tuple-element.21), channel_id=1, source_target_pairs={{4,0},{8,4},{12,8},{16,12},{20,16},{24,20},{28,24},{5,1},{9,5},{13... | collective-permute-start | bytes 196616 | tf_op jit(solution)/shard_map/ppermute | solution.py:22
  27.2 0.6 copy-start.7
  32.0 1.2 copy-start.6
  35.1 0.9 copy-start.5
  36.0 1.6 copy-start.10
  36.0 1.8 copy-start.12
  37.6 197.9 %all-gather.6.cloned.1.call-start = ((), (), s32[]{:S(2)}) async-start(), calls=%async_computation.3 | async-start | bytes 15728640 | tf_op jit(solution)/shard_map/all_gather | solution.py:135
  37.8 30.6 %copy-start.3 = (s32[768,2]{1,0:T(8,128)}, s32[768,2]{1,0:T(8,128)S(1)}, u32[]{:S(2)}) copy-start(s32[768,2]{1,0:T(8,128)S(1)} %copy.59) | copy-start | bytes 18436
  68.5 0.8 copy-start.9
  70.1 1.7 copy-start
  155.1 146.7 %all-gather.8.cloned.1.call-start = ((), (), s32[]{:S(2)}) async-start(), calls=%async_computation.4 | async-start | bytes 7864320 | tf_op jit(solution)/shard_map/all_gather | solution.py:146
  235.5 6.5 %copy-start.14 = (bf16[4,2048,256]{2,1,0:T(8,128)(2,1)S(1)}, bf16[4,2048,256]{2,1,0:T(8,128)(2,1)}, u32[]{:S(2)}) copy-start(bf16[4,2048,256]{2,1,0:T(8,128)(2,1)} %param.26) | copy-start | bytes 12582916
  311.3 6.1 %copy-start.4 = (s32[768,2]{1,0:T(8,128)S(1)}, s32[768,2]{1,0:T(8,128)}, u32[]{:S(2)}) copy-start(s32[768,2]{1,0:T(8,128)} %copy-done.3) | copy-start | bytes 18436
  311.3 6.9 %copy-start.11 = (f32[768,2]{0,1:T(2,128)S(1)}, f32[768,2]{0,1:T(2,128)}, u32[]{:S(2)}) copy-start(f32[768,2]{0,1:T(2,128)} %param.25) | copy-start | bytes 18436
  311.3 76.9 %all-to-all-start.1 = ((bf16[4,8,96,512]{3,2,0,1:T(8,128)(2,1)}), bf16[4,8,96,512]{3,2,0,1:T(8,128)(2,1)}, u32[]{:S(2)}, u32[]{:S(2)}) async-start(bf16[4,8,96,512]{3,2,0,1:T(8,128)(2,1)} %copy.65), calls=%async_computation.1 | async-start | bytes 6291456 | tf_op jit(solution)/shard_map/all_to_all | solution.py:150
  400.6 7.3 %copy-start.1 = (bf16[768,2048]{1,0:T(8,128)(2,1)S(1)}, bf16[768,2048]{1,0:T(8,128)(2,1)}, u32[]{:S(2)}) copy-start(bf16[768,2048]{1,0:T(8,128)(2,1)} %copy-done) | copy-start | bytes 9437188
  406.7 1.2 copy-start.2
  407.9 6.5 %copy-start.13 = (f32[512]{0:T(512)S(1)}, f32[512]{0:T(512)}, u32[]{:S(2)}) copy-start(f32[512]{0:T(512)} %param.29) | copy-start | bytes 6148
Sparse Core Ops, SparseCore 0:
  37.7 22.9 all-gather.3
  155.2 80.1 all-gather.5
  254.6 47.1 all-gather.7
where the time goes:
time: 424 us
  waiting for transfers between devices  212 us (50%)
  blocking collectives  82.6 us (19%)
  local copies, waits for them, and re-layouts  45.3 us (11%)
  matrix products  31.6 us (7%)
  other arithmetic  20.2 us (5%)
  starting transfers between devices  18 us (4%)
  between operations  13.7 us (3%)
    all_gather x1, waiting for transfers between devices, shards(): arrived = lax.all_gather(received, 'tp', axis=2, tiled=True)  80.1 us
    all_to_all x1, blocking collectives, shards(): lax.all_to_all(outgoing, 'sp', split_axis=1, concat_axis=1, tiled=True)  76.5 us
    all_to_all x1, waiting for transfers between devices, shards(): lax.all_to_all(produced.reshape(experts_local, sp_size, tp_size * capacit...  69.8 us
    all_gather x1, waiting for transfers between devices, shards(): lax.all_gather(hidden, 'tp', axis=2, tiled=True)  47.3 us
    all_gather x1, waiting for transfers between devices, shards(): lax.all_gather(attended, 'tp', axis=1, tiled=True)  14.9 us
    ppermute x2, starting transfers between devices, with_halo(): lax.ppermute(lax.slice_in_dim(block, block.shape[dim] - width, None, axis...  9.4 us
  transfers between devices with their start and end apart: 8, of which 4 were waited for; matrix products, arithmetic and copies ran while one was open for 4% of the time, Pallas kernels for 0%

commit v1 on v0

--- a/solution.py
+++ b/solution.py
@@ -132,7 +132,8 @@
     source = jnp.full((slot_count,), row_count, jnp.int32).at[own_slots].set(own_rows)
     outgoing = extended[source].reshape(experts_local, sp_size, capacity, width)
     received = lax.all_to_all(outgoing, "sp", split_axis=1, concat_axis=1, tiled=True)
-    arrived = lax.all_gather(received, "tp", axis=2, tiled=True)
+    outgoing_2 = jnp.stack([received] * lax.axis_size("tp"))
+    arrived = jnp.concatenate(lax.all_to_all(outgoing_2, "tp", 0, 0), axis=2)
     expert_rows = arrived.reshape(experts_local, sp_size * tp_size * capacity, width)
     gate_part = jnp.einsum(
         "esd,edf->esf", expert_rows, gate_weight, preferred_element_type=jnp.float32

time: 424 us -> 487 us (1.15)
  blocking collectives: 82.6 us -> 225 us
  waiting for transfers between devices: 212 us -> 130 us
    all_to_all x0 -> x1, blocking collectives: none -> 142 us  [shards(): arrived = jnp.concatenate(lax.all_to_all(outgoing_2, 'tp', 0, 0), axis=2)]
    all_gather x1 -> x0, waiting for transfers between devices: 80.1 us -> none  [shards(): arrived = lax.all_gather(received, 'tp', axis=2, tiled=True)]
    all_gather x1 -> x0, local copies, waits for them, and re-layouts: 6.44 us -> none  [shards(): arrived = lax.all_gather(received, 'tp', axis=2, tiled=True)]
    another operation x2 -> x3, local copies, waits for them, and re-layouts: 0.01 us -> 6.18 us  [the longest x1 6.17 us: shards(): outgoing_2 = jnp.stack([received] * lax.axis_size('tp'))]
  transfers between devices with their start and end apart: 8 -> 7, of which waited for: 4 -> 3; matrix products, arithmetic and copies ran while one was open for 4% -> 4% of each run, Pallas kernels for 0% -> 0%
where the time goes in v1:
time: 487 us; the launch traced here: 486 us
  blocking collectives  225 us (46%)
  waiting for transfers between devices  130 us (27%)
  local copies, waits for them, and re-layouts  47.4 us (10%)
  matrix products  31.6 us (6%)
  other arithmetic  20.2 us (4%)
  starting transfers between devices  17.7 us (4%)
  between operations  14 us (3%)
    all_to_all x1, blocking collectives, shards(): arrived = jnp.concatenate(lax.all_to_all(outgoing_2, 'tp', 0, 0), axis=2)  142 us
    all_to_all x1, blocking collectives, shards(): lax.all_to_all(outgoing, 'sp', split_axis=1, concat_axis=1, tiled=True)  76.4 us
    all_to_all x1, waiting for transfers between devices, shards(): lax.all_to_all(produced.reshape(experts_local, sp_size, tp_size * capacit...  69.8 us
    all_gather x1, waiting for transfers between devices, shards(): lax.all_gather(hidden, 'tp', axis=2, tiled=True)  45.5 us
    all_gather x1, waiting for transfers between devices, shards(): lax.all_gather(attended, 'tp', axis=1, tiled=True)  14.9 us
  transfers between devices with their start and end apart: 7, of which 3 were waited for; matrix products, arithmetic and copies ran while one was open for 4% of the time, Pallas kernels for 0%

profile of v1, /device:TPU:0, one launch (start us, length us, event | category | flops | bytes accessed | tf_op | source)
XLA Modules:
  0.0 486.1 jit_solution(6045757087814694851)
XLA Ops:
  6.6 0.8 fusion.54
  7.4 4.9 collective-permute-start.1
  12.3 1.3 collective-permute-start.3
  13.6 1.0 constant_dynamic-update-slice_fusion.1
  14.5 1.0 constant_dynamic-update-slice_fusion
  15.5 0.6 fusion.52
  16.1 4.5 collective-permute-start
  20.7 1.3 collective-permute-start.2
  22.0 0.7 slice.96
  22.7 0.8 fusion.55
  23.5 1.1 fusion.51
  24.8 0.8 copy.52
  25.9 0.7 and_and_fusion.2
  27.2 0.6 copy-done.7
  27.8 1.5 pad_maximum_fusion.3
  29.4 1.0 copy.47
  30.4 0.8 copy.46
  33.2 0.8 convolution_convert_fusion.3
  35.1 0.8 convolution_convert_fusion.2
  36.0 0.7 convolution_convert_fusion.1
  36.8 0.8 pad_maximum_fusion
  38.5 3.5 reduce-window.6
  42.6 3.1 scatter_custom_fusion
  45.7 14.9 %all-gather.3.cloned.1.call-done = bf16[768,1024]{0,1:T(8,128)(2,1)} async-done(((bf16[768,256]{0,1:T(8,128)(2,1)}), bf16[768,1024]{0,1:T(8,128)(2,1)}) %all-gather.3.cloned.1.call-update) | async-done | bytes 1572880 | tf_op jit(solution)/shard_map/all_gather | solution.py:102
  60.6 7.8 %fusion.56 = (f32[768]{0:T(1024)S(1)}, f32[768,2048]{1,0:T(8,128)S(1)}) fusion(bf16[768,1024]{0,1:T(8,128)(2,1)} %all-gather.3.cloned.1.call-done, bf16[1024,2048]{1,0:T(8,128)(2,1)} %param.21, bf16[768,2048]{1,0:T(8,128)(2,1)} %param.15), kind=kOutput, calls=%fused_computation.146 | convolution fusion | flops 3227516160 | bytes 15207424 | tf_op jit(solution)/shard_map/dot_general | solution.py:101
  68.5 0.8 multiply_reduce_fusion
  69.2 0.9 multiply_convert_fusion
  70.1 1.7 copy-done
  72.0 4.3 gather_fusion
  76.3 2.3 copy.63
  78.6 76.4 %all_to_all.15 = bf16[4,8,24,2048]{3,2,0,1:T(8,128)(2,1)S(1)} all-to-all(bf16[4,8,24,2048]{3,2,0,1:T(8,128)(2,1)S(1)} %copy.63), channel_id=1, replica_groups=mesh['sp'=8,'tp'=4] {'sp'}, dimensions={1} | all-to-all | bytes 6291456 | tf_op jit(solution)/shard_map/all_to_all | solution.py:134
  155.2 6.2 %stack.2 = bf16[4,4,8,24,2048]{4,3,2,1,0:T(8,128)(2,1)} broadcast(bf16[4,8,24,2048]{3,2,1,0:T(8,128)(2,1)S(1)} %copy.64), dimensions={1,2,3,4} | broadcast | bytes 15728640 | tf_op jit(solution)/shard_map/stack | solution.py:135
  161.4 142.4 %all_to_all.16 = bf16[4,4,8,24,2048]{4,3,2,1,0:T(8,128)(2,1)S(1)} all-to-all(bf16[4,4,8,24,2048]{4,3,2,1,0:T(8,128)(2,1)} %stack.2), channel_id=1, replica_groups=mesh['sp'=8,'tp'=4] {'tp'}, dimensions={0} | all-to-all | bytes 25165824 | tf_op jit(solution)/shard_map/all_to_all | solution.py:136
  303.8 1.9 copy.65
  306.0 5.2 %fusion.57 = f32[4,768,256]{2,1,0:T(8,128)} fusion(bf16[4,768,2048]{2,1,0:T(8,128)(2,1)S(1)} %bitcast.122, bf16[4,2048,256]{2,1,0:T(8,128)(2,1)S(1)} %copy-done.14), kind=kOutput, calls=%fused_computation.147 | convolution fusion | flops 3221225472 | bytes 19922944 | tf_op jit(solution)/shard_map/esd,edf->esf/dot_general | solution.py:138
  311.2 7.4 %multiply_convert_fusion.1 = bf16[4,768,256]{2,1,0:T(8,128)(2,1)} fusion(f32[4,768,256]{2,1,0:T(8,128)} %fusion.57, bf16[4,768,2048]{2,1,0:T(8,128)(2,1)S(1)} %bitcast.123, bf16[4,2048,256]{2,1,0:T(8,128)(2,1)} %param.27), kind=kOutput, calls=%fused_computation.7 | convolution fusion | flops 3225944064 | bytes 21495808 | tf_op jit(solution)/shard_map/esd,edf->esf/dot_general | solution.py:141
  318.6 45.5 %all-gather.5.cloned.1.call-done = bf16[4,768,1024]{2,1,0:T(8,128)(2,1)} async-done(((bf16[4,768,256]{2,1,0:T(8,128)(2,1)}), bf16[4,768,1024]{2,1,0:T(8,128)(2,1)}) %all-gather.5.cloned.1.call-update) | async-done | bytes 6291472 | tf_op jit(solution)/shard_map/all_gather | solution.py:147
  364.1 7.4 %convolution_convert_fusion = bf16[4,768,512]{2,1,0:T(8,128)(2,1)S(1)} fusion(bf16[4,768,1024]{2,1,0:T(8,128)(2,1)} %all-gather.5.cloned.1.call-done, bf16[4,1024,512]{2,1,0:T(8,128)(2,1)} %param.28), kind=kOutput, calls=%fused_computation.8 | convolution fusion | flops 3222798336 | bytes 13631488 | tf_op jit(solution)/shard_map/esf,efc->esc/dot_general | solution.py:145
  371.5 2.0 copy.66
  373.5 5.6 %all-to-all-start.2 = ((bf16[4,8,96,512]{3,2,0,1:T(8,128)(2,1)}), bf16[4,8,96,512]{3,2,0,1:T(8,128)(2,1)}, u32[]{:S(2)}, u32[]{:S(2)}) async-start(bf16[4,8,96,512]{3,2,0,1:T(8,128)(2,1)} %copy.66), calls=%async_computation.2 | async-start | bytes 6291456 | tf_op jit(solution)/shard_map/all_to_all | solution.py:151
  380.6 69.8 %all-to-all-done.2 = bf16[4,8,96,512]{3,2,0,1:T(8,128)(2,1)} async-done(((bf16[4,8,96,512]{3,2,0,1:T(8,128)(2,1)}), bf16[4,8,96,512]{3,2,0,1:T(8,128)(2,1)}, u32[]{:S(2)}, u32[]{:S(2)}) %all-to-all-start.2) | async-done | bytes 3145760 | tf_op jit(solution)/shard_map/all_to_all | solution.py:151
  450.4 2.2 copy.67
  452.6 5.4 %gather_fusion.1 = bf16[1536,512]{1,0:T(8,128)(2,1)} fusion(bf16[3072,512]{1,0:T(8,128)(2,1)S(1)} %bitcast.120, s32[2048]{0:T(1024)S(1)} %pad_clamp_fusion), kind=kCustom, calls=%fused_computation.1 | custom fusion | bytes 3151872 | tf_op jit(solution)/shard_map/gather | solution.py:159
  458.0 4.7 reshape.240
  462.8 6.1 %multiply_reduce_fusion.1 = f32[768,512]{1,0:T(8,128)S(1)} fusion(f32[768,2,512]{2,1,0:T(2,128)} %reshape.240, f32[768,2]{1,0:T(8,128)S(1)} %copy.58), kind=kLoop, calls=%fused_computation.6 | loop fusion | flops 1179648 | bytes 4724736 | tf_op jit(solution)/shard_map/reduce_sum | solution.py:160
  468.9 1.1 copy-done.2
  470.5 6.1 %all-reduce.1 = (f32[768]{0:T(1024)S(1)}, f32[768]{0:T(1024)S(1)}) all-reduce(f32[768]{0:T(1024)S(1)} %get-tuple-element.6, f32[768]{0:T(1024)S(1)} %get-tuple-element.5), channel_id=1, replica_groups=mesh['sp'=8,'tp'=4] {'tp'}, use_global_device_ids=true, to_apply=%region_16.17 | all-reduce | flops 1536 | bytes 12288 | tf_op jit(solution)/shard_map/psum | solution.py:164
  476.6 2.6 multiply_convert_fusion.2
  (97 shorter events, 8.4 us)
Async XLA Ops:
  6.5 19.4 %copy-start.8 = (s32[768]{0:T(1024)S(1)}, s32[768]{0:T(1024)}, u32[]{:S(2)}) copy-start(s32[768]{0:T(1024)} %param.19) | copy-start | bytes 9220
  6.5 18.1 %slice-start = ((bf16[768,128]{1,0:T(8,128)(2,1)}), bf16[512,128]{1,0:T(8,128)(2,1)S(1)}, s32[]{:S(2)}) async-start(bf16[768,128]{1,0:T(8,128)(2,1)} %param.17), calls=%async_computation.5 | async-start | bytes 262144 | tf_op jit(solution)/shard_map/slice | solution.py:75
  6.5 18.3 %slice-start.1 = ((bf16[768,128]{1,0:T(8,128)(2,1)}), bf16[512,128]{1,0:T(8,128)(2,1)S(1)}, s32[]{:S(2)}) async-start(bf16[768,128]{1,0:T(8,128)(2,1)} %param.18), calls=%async_computation.6 | async-start | bytes 262144 | tf_op jit(solution)/shard_map/slice | solution.py:76
  6.5 18.0 %copy-start.15 = (f32[4]{0:T(128)S(1)}, f32[4]{0:T(128)}, u32[]{:S(2)}) copy-start(f32[4]{0:T(128)} %param.20) | copy-start | bytes 52
  6.5 54.1 %all-gather.3.cloned.1.call-start = ((), (), s32[]{:S(2)}) async-start(), calls=%async_computation.3 | async-start | bytes 1966080 | tf_op jit(solution)/shard_map/all_gather | solution.py:102
  7.4 18.5 %collective-permute-start.1 = (s32[128]{0:T(128)S(1)}, s32[128]{0:T(128)S(1)}, u32[]{:S(2)}, u32[]{:S(2)}) collective-permute-start(s32[128]{0:T(128)S(1)} %get-tuple-element.30), channel_id=1, source_target_pairs={{0,4},{4,8},{8,12},{12,16},{16,20},{20,24},{24,28},{1,5},{5,9},{9,... | collective-permute-start | bytes 1544 | tf_op jit(solution)/shard_map/ppermute | solution.py:19
  12.3 13.6 %collective-permute-start.3 = (s32[128]{0:T(128)S(1)}, s32[128]{0:T(128)S(1)}, u32[]{:S(2)}, u32[]{:S(2)}) collective-permute-start(s32[128]{0:T(128)S(1)} %get-tuple-element.31), channel_id=1, source_target_pairs={{4,0},{8,4},{12,8},{16,12},{20,16},{24,20},{28,24},{5,1},{9,5},{13... | collective-permute-start | bytes 1544 | tf_op jit(solution)/shard_map/ppermute | solution.py:22
  16.1 11.1 %collective-permute-start = (bf16[128,256]{1,0:T(8,128)(2,1)}, bf16[128,256]{1,0:T(8,128)(2,1)S(1)}, u32[]{:S(2)}, u32[]{:S(2)}) collective-permute-start(bf16[128,256]{1,0:T(8,128)(2,1)} %get-tuple-element.20), channel_id=1, source_target_pairs={{0,4},{4,8},{8,12},{12,16},{16,20},{20,24},{24,28},{1,5},{5,9},{9,... | collective-permute-start | bytes 196616 | tf_op jit(solution)/shard_map/ppermute | solution.py:19
  20.7 7.2 %collective-permute-start.2 = (bf16[128,256]{1,0:T(8,128)(2,1)S(1)}, bf16[128,256]{1,0:T(8,128)(2,1)}, u32[]{:S(2)}, u32[]{:S(2)}) collective-permute-start(bf16[128,256]{1,0:T(8,128)(2,1)S(1)} %get-tuple-element.21), channel_id=1, source_target_pairs={{4,0},{8,4},{12,8},{16,12},{20,16},{24,20},{28,24},{5,1},{9,5},{13... | collective-permute-start | bytes 196616 | tf_op jit(solution)/shard_map/ppermute | solution.py:22
  27.2 0.6 copy-start.7
  32.0 1.2 copy-start.6
  35.1 0.9 copy-start.5
  36.0 1.6 copy-start.10
  36.0 1.8 copy-start.12
  37.6 326.5 %all-gather.5.cloned.1.call-start = ((), (), s32[]{:S(2)}) async-start(), calls=%async_computation.4 | async-start | bytes 7864320 | tf_op jit(solution)/shard_map/all_gather | solution.py:147
  37.8 30.6 %copy-start.3 = (s32[768,2]{1,0:T(8,128)}, s32[768,2]{1,0:T(8,128)S(1)}, u32[]{:S(2)}) copy-start(s32[768,2]{1,0:T(8,128)S(1)} %copy.59) | copy-start | bytes 18436
  68.5 0.8 copy-start.9
  70.1 1.7 copy-start
  303.8 2.2 copy-start.14
  373.5 6.1 %copy-start.4 = (s32[768,2]{1,0:T(8,128)S(1)}, s32[768,2]{1,0:T(8,128)}, u32[]{:S(2)}) copy-start(s32[768,2]{1,0:T(8,128)} %copy-done.3) | copy-start | bytes 18436
  373.5 6.9 %copy-start.11 = (f32[768,2]{0,1:T(2,128)S(1)}, f32[768,2]{0,1:T(2,128)}, u32[]{:S(2)}) copy-start(f32[768,2]{0,1:T(2,128)} %param.25) | copy-start | bytes 18436
  373.5 76.9 %all-to-all-start.2 = ((bf16[4,8,96,512]{3,2,0,1:T(8,128)(2,1)}), bf16[4,8,96,512]{3,2,0,1:T(8,128)(2,1)}, u32[]{:S(2)}, u32[]{:S(2)}) async-start(bf16[4,8,96,512]{3,2,0,1:T(8,128)(2,1)} %copy.66), calls=%async_computation.2 | async-start | bytes 6291456 | tf_op jit(solution)/shard_map/all_to_all | solution.py:151
  462.8 7.3 %copy-start.1 = (bf16[768,2048]{1,0:T(8,128)(2,1)S(1)}, bf16[768,2048]{1,0:T(8,128)(2,1)}, u32[]{:S(2)}) copy-start(bf16[768,2048]{1,0:T(8,128)(2,1)} %copy-done) | copy-start | bytes 9437188
  468.9 1.2 copy-start.2
  470.1 6.5 %copy-start.13 = (f32[512]{0:T(512)S(1)}, f32[512]{0:T(512)}, u32[]{:S(2)}) copy-start(f32[512]{0:T(512)} %param.29) | copy-start | bytes 6148
Sparse Core Ops, SparseCore 0:
  37.7 22.9 all-gather.2
  318.7 45.3 all-gather.4
